TPU v7x, 32 devices: a whole 2x2x4 slice. The times are simulated.
32 devices in a mesh: sp: 8 (over z, y), tp: 4 (over x, core).
Axes of the slice: x: 2, y: 2, z: 4, core: 2. Of those that a mesh axis runs over, the one named last changes fastest.
Arguments:
- residual: bfloat16 [6144, 2048], P(('sp', 'tp')), may hold values from -6 to 6
- queries: bfloat16 [6144, 1024], P('sp', 'tp'), may hold values from -240 to 240
- keys: bfloat16 [6144, 256], P('sp', 'tp'), may hold values from -6 to 6
- values: bfloat16 [6144, 256], P('sp', 'tp'), may hold values from -18 to 18
- sinks: float32 [16], P('tp'), may hold values from 1 to 6
- out_weight: bfloat16 [1024, 2048], replicated, may hold values from -0.5625 to 0.5625
- norm_gain: float32 [2048], replicated, may hold values from 0.1 to 1.9
- gate_weight: bfloat16 [2048, 5632], P('sp', 'tp'), may hold values from -0.125 to 0.125
- up_weight: bfloat16 [2048, 5632], P('sp', 'tp'), may hold values from -0.125 to 0.125
- down_weight: bfloat16 [5632, 2048], P('tp', 'sp'), may hold values from -0.078125 to 0.078125
Outputs:
- layer_out: bfloat16 [6144, 2048], P(('sp', 'tp'))
All inputs are finite; a program needn't handle non-finite values.
Results may differ from a plain program's by a relative error of at most 0.014.
Values may be sent and summed in bfloat16 or wider, within the bound.
A program may use at most 128 MiB of HBM per device.

v0:
```python
import jax
import jax.numpy as jnp
from jax import lax
from jax.sharding import PartitionSpec as P

HEAD = 64
WINDOW = 128


def passed_along(block, axis, distance):
    devices = range(lax.axis_size(axis))
    route = [(i - distance, i) for i in devices if i - distance in devices]
    return lax.ppermute(block, axis, route)


def attend(queries, keys_ext, values_ext, sinks, block_base):
    rows = queries.shape[0]
    nblk = rows // WINDOW
    qheads = sinks.shape[0]
    kheads = keys_ext.shape[1] // HEAD
    group = qheads // kheads
    qblock = queries.reshape(nblk, WINDOW, kheads, group, HEAD).astype(jnp.float32)

    def band(arr):
        first = arr[:rows].reshape(nblk, WINDOW, kheads, HEAD)
        second = arr[WINDOW:].reshape(nblk, WINDOW, kheads, HEAD)
        return jnp.concatenate([first, second], axis=1).astype(jnp.float32)

    kband = band(keys_ext)
    vband = band(values_ext)
    score = jnp.einsum("nqhgd,nkhd->nhgqk", qblock, kband) * HEAD ** (-0.5)
    qidx = jnp.arange(WINDOW)[:, None]
    kidx = jnp.arange(2 * WINDOW)[None, :]
    rel = qidx + WINDOW - kidx
    valid = (rel >= 0) & (rel < WINDOW)
    blocks = block_base + jnp.arange(nblk)
    valid = valid[None] & ((blocks > 0)[:, None, None] | (kidx >= WINDOW)[None])
    score = jnp.where(valid[:, None, None], score, -jnp.inf)
    sink = sinks.reshape(kheads, group)[None, :, :, None]
    top = jnp.maximum(jnp.max(score, axis=-1), sink)
    expd = jnp.exp(score - top[..., None])
    denom = jnp.sum(expd, axis=-1) + jnp.exp(sink - top)
    weights = (expd / denom[..., None]).astype(jnp.bfloat16)
    result = jnp.einsum("nhgqk,nkhd->nqhgd", weights.astype(jnp.float32), vband)
    return result.reshape(rows, qheads * HEAD).astype(jnp.bfloat16)


def shards(
    residual,
    queries,
    keys,
    values,
    sinks,
    out_weight,
    norm_gain,
    gate_weight,
    up_weight,
    down_weight,
):
    rows_dev = queries.shape[0]
    prev_keys, prev_values = passed_along((keys[-WINDOW:], values[-WINDOW:]), "sp", 1)
    keys_ext = jnp.concatenate([prev_keys, keys], axis=0)
    values_ext = jnp.concatenate([prev_values, values], axis=0)
    attention = attend(
        queries, keys_ext, values_ext, sinks, lax.axis_index("sp") * (rows_dev // WINDOW)
    )
    width = attention.shape[1]
    mine = lax.dynamic_slice_in_dim(out_weight, lax.axis_index("tp") * width, width, 0)
    proj = lax.psum_scatter(
        jnp.dot(attention, mine, preferred_element_type=jnp.float32).astype(jnp.bfloat16),
        "tp",
        scatter_dimension=0,
        tiled=True,
    ).astype(jnp.float32)
    mixed = (residual.astype(jnp.float32) + proj).astype(jnp.bfloat16)
    mixf = mixed.astype(jnp.float32)
    normed = (
        mixf * lax.rsqrt(jnp.mean(mixf * mixf, axis=-1, keepdims=True) + 1e-06) * norm_gain
    ).astype(jnp.bfloat16)
    normed_all = lax.all_gather(normed, "tp", axis=0, tiled=True)
    gate = jnp.dot(
        normed_all,
        lax.all_gather(gate_weight, "sp", axis=0, tiled=True),
        preferred_element_type=jnp.float32,
    )
    upper = jnp.dot(
        normed_all,
        lax.all_gather(up_weight, "sp", axis=0, tiled=True),
        preferred_element_type=jnp.float32,
    )
    hidden = (jax.nn.silu(gate) * upper).astype(jnp.bfloat16)
    terms = jnp.dot(
        hidden,
        lax.all_gather(down_weight, "sp", axis=1, tiled=True),
        preferred_element_type=jnp.float32,
    )
    ffn = lax.psum_scatter(
        terms.astype(jnp.bfloat16), "tp", scatter_dimension=0, tiled=True
    ).astype(jnp.float32)
    return (mixed.astype(jnp.float32) + ffn).astype(jnp.bfloat16)


def solution(mesh):
    placed = (
        P(("sp", "tp"), None),
        P("sp", "tp"),
        P("sp", "tp"),
        P("sp", "tp"),
        P("tp"),
        P(),
        P(),
        P("sp", "tp"),
        P("sp", "tp"),
        P("tp", "sp"),
    )
    return jax.shard_map(
        shards, mesh=mesh, in_specs=placed, out_specs=P(("sp", "tp"), None), check_vma=False
    )
```

profile of v0, /device:TPU:0, one launch (start us, length us, event | category | flops | bytes accessed | tf_op | source)
XLA Modules:
  0.0 407.9 jit_solution(3157988359120101178)
XLA Ops:
  7.4 0.7 slice.14
  8.1 4.9 %collective-permute-start.1 = (bf16[128,64]{0,1:T(8,128)(2,1)S(1)}, bf16[128,64]{0,1:T(8,128)(2,1)S(1)}, u32[]{:S(2)}, u32[]{:S(2)}) collective-permute-start(bf16[128,64]{0,1:T(8,128)(2,1)S(1)} %slice.14), channel_id=1, source_target_pairs={{0,4},{4,8},{8,12},{12,16},{16,20},{20,24},{24,28},{1,5},{5,9},{9,... | collective-permute-start | bytes 49160 | tf_op jit(solution)/shard_map/ppermute | solution.py:13
  13.0 0.7 slice.12
  13.7 3.4 collective-permute-start
  17.6 1.0 reshape.145
  18.6 1.0 reshape.142
  19.6 2.5 reshape.151
  22.9 0.9 pad_maximum_fusion
  23.9 1.9 fusion.1
  25.9 0.7 fusion
  27.3 1.0 reshape.141
  28.4 1.8 fusion.12
  30.5 4.0 convolution_convert_fusion
  35.1 37.7 %reduce-scatter.3.cloned.1.call-done = bf16[192,2048]{1,0:T(8,128)(2,1)} async-done(((bf16[768,2048]{1,0:T(8,128)(2,1)}), bf16[192,2048]{1,0:T(8,128)(2,1)}) %reduce-scatter.3.cloned.1.call-update) | async-done | bytes 786448 | tf_op jit(solution)/shard_map/reduce_scatter | solution.py:69
  72.8 1.5 fusion.2
  74.3 2.3 fusion.4
  78.2 51.4 %all-gather.7.cloned.1.call-done = bf16[2048,1408]{1,0:T(8,128)(2,1)} async-done(((bf16[256,1408]{1,0:T(8,128)(2,1)}), bf16[2048,1408]{1,0:T(8,128)(2,1)}) %all-gather.7.cloned.1.call-update) | async-done | bytes 5767184 | tf_op jit(solution)/shard_map/all_gather | solution.py:83
  129.6 28.0 %all-gather.5.cloned.1.call-done = bf16[768,2048]{1,0:T(8,128)(2,1)} async-done(((bf16[192,2048]{1,0:T(8,128)(2,1)}), bf16[768,2048]{1,0:T(8,128)(2,1)}) %all-gather.5.cloned.1.call-update) | async-done | bytes 3145744 | tf_op jit(solution)/shard_map/all_gather | solution.py:80
  157.6 9.7 %fusion.33 = f32[768,1408]{1,0:T(8,128)} fusion(bf16[768,2048]{1,0:T(8,128)(2,1)} %all-gather.5.cloned.1.call-done, bf16[2048,1408]{1,0:T(8,128)(2,1)} %all-gather.7.cloned.1.call-done), kind=kOutput, calls=%fused_computation.52 | convolution fusion | flops 4429185024 | bytes 13238272 | tf_op jit(solution)/shard_map/dot_general | solution.py:81
  167.2 85.1 %all-gather.11.cloned.1.call-done = bf16[1408,2048]{1,0:T(8,128)(2,1)} async-done(((bf16[1408,256]{1,0:T(8,128)(2,1)}), bf16[1408,2048]{1,0:T(8,128)(2,1)}) %all-gather.11.cloned.1.call-update) | async-done | bytes 5767184 | tf_op jit(solution)/shard_map/all_gather | solution.py:94
  252.4 92.5 %all-gather.9.cloned.1.call-done = bf16[2048,1408]{1,0:T(8,128)(2,1)} async-done(((bf16[256,1408]{1,0:T(8,128)(2,1)}), bf16[2048,1408]{1,0:T(8,128)(2,1)}) %all-gather.9.cloned.1.call-update) | async-done | bytes 5767184 | tf_op jit(solution)/shard_map/all_gather | solution.py:88
  344.9 16.8 %convolution_convert_fusion.1 = bf16[768,2048]{1,0:T(8,128)(2,1)} fusion(bf16[1408,2048]{1,0:T(8,128)(2,1)} %all-gather.11.cloned.1.call-done, f32[768,1408]{1,0:T(8,128)} %fusion.33, bf16[768,2048]{1,0:T(8,128)(2,1)} %all-gather.5.cloned.1.call-done, bf16[2048,1408]{1,0:T(8,128)(2,1)} %all-gather.9.cloned.1.call-done), kind=kOutput, calls=%fused_computation.2 | convolution fusion | flops 8866430976 | bytes 22151168 | tf_op jit(solution)/shard_map/dot_general | solution.py:92
  361.7 36.2 %reduce-scatter.5.cloned.1.call-done = bf16[192,2048]{1,0:T(8,128)(2,1)} async-done(((bf16[768,2048]{1,0:T(8,128)(2,1)}), bf16[192,2048]{1,0:T(8,128)(2,1)}) %reduce-scatter.5.cloned.1.call-update) | async-done | bytes 786448 | tf_op jit(solution)/shard_map/reduce_scatter | solution.py:97
  397.9 2.4 fusion.5
  (40 shorter events, 4.5 us)
Async XLA Ops:
  7.4 65.4 %reduce-scatter.3.cloned.1.call-start = ((), (), s32[]{:S(2)}) async-start(), calls=%async_computation.2 | async-start | bytes 3932160 | tf_op jit(solution)/shard_map/reduce_scatter | solution.py:69
  8.1 14.8 %collective-permute-start.1 = (bf16[128,64]{0,1:T(8,128)(2,1)S(1)}, bf16[128,64]{0,1:T(8,128)(2,1)S(1)}, u32[]{:S(2)}, u32[]{:S(2)}) collective-permute-start(bf16[128,64]{0,1:T(8,128)(2,1)S(1)} %slice.14), channel_id=1, source_target_pairs={{0,4},{4,8},{8,12},{12,16},{16,20},{20,24},{24,28},{1,5},{5,9},{9,... | collective-permute-start | bytes 49160 | tf_op jit(solution)/shard_map/ppermute | solution.py:13
  13.7 13.0 %collective-permute-start = (bf16[128,64]{0,1:T(8,128)(2,1)S(1)}, bf16[128,64]{0,1:T(8,128)(2,1)S(1)}, u32[]{:S(2)}, u32[]{:S(2)}) collective-permute-start(bf16[128,64]{0,1:T(8,128)(2,1)S(1)} %slice.12), channel_id=1, source_target_pairs={{0,4},{4,8},{8,12},{12,16},{16,20},{20,24},{24,28},{1,5},{5,9},{9,... | collective-permute-start | bytes 49160 | tf_op jit(solution)/shard_map/ppermute | solution.py:13
  19.6 6.2 %copy-start.4 = (f32[4]{0:T(128)S(1)}, f32[4]{0:T(128)}, u32[]{:S(2)}) copy-start(f32[4]{0:T(128)} %param.14) | copy-start | bytes 52
  23.9 2.8 copy-start.2
  34.5 38.3 %copy-start = (bf16[192,2048]{1,0:T(8,128)(2,1)S(1)}, bf16[192,2048]{1,0:T(8,128)(2,1)}, u32[]{:S(2)}) copy-start(bf16[192,2048]{1,0:T(8,128)(2,1)} %param.10) | copy-start | bytes 2359300
  34.5 39.8 %copy-start.3 = (f32[2048]{0:T(1024)S(1)}, f32[2048]{0:T(1024)}, u32[]{:S(2)}) copy-start(f32[2048]{0:T(1024)} %param.16) | copy-start | bytes 24580
  34.5 95.1 %all-gather.7.cloned.1.call-start = ((), (), s32[]{:S(2)}) async-start(), calls=%async_computation.4 | async-start | bytes 6488064 | tf_op jit(solution)/shard_map/all_gather | solution.py:83
  35.1 122.5 %all-gather.5.cloned.1.call-start = ((), (), s32[]{:S(2)}) async-start(), calls=%async_computation.3 | async-start | bytes 3932160 | tf_op jit(solution)/shard_map/all_gather | solution.py:80
  76.6 175.8 %all-gather.11.cloned.1.call-start = ((), (), s32[]{:S(2)}) async-start(), calls=%async_computation.6 | async-start | bytes 6488064 | tf_op jit(solution)/shard_map/all_gather | solution.py:94
  77.2 267.7 %all-gather.9.cloned.1.call-start = ((), (), s32[]{:S(2)}) async-start(), calls=%async_computation.5 | async-start | bytes 6488064 | tf_op jit(solution)/shard_map/all_gather | solution.py:88
  77.9 320.0 %reduce-scatter.5.cloned.1.call-start = ((), (), s32[]{:S(2)}) async-start(), calls=%async_computation.7 | async-start | bytes 3932160 | tf_op jit(solution)/shard_map/reduce_scatter | solution.py:97
  361.7 36.2 %copy-start.1 = (bf16[192,2048]{1,0:T(8,128)(2,1)S(1)}, bf16[192,2048]{1,0:T(8,128)(2,1)}, u32[]{:S(2)}) copy-start(bf16[192,2048]{1,0:T(8,128)(2,1)} %reduce-scatter.3.cloned.1.call-done) | copy-start | bytes 2359300
Sparse Core Ops, SparseCore 0:
  34.6 38.1 reduce-scatter.2
  361.9 35.9 reduce-scatter.4
Sparse Core Ops, SparseCore 1:
  37.2 92.4 all-gather.6
  131.0 26.5 all-gather.4
  159.5 92.9 all-gather.10
  254.6 90.3 all-gather.8
where the time goes:
time: 409 us; the launch traced here: 408 us
  waiting for transfers between devices  333 us (81%)
  matrix products  34.1 us (8%)
  between operations  15.2 us (4%)
  other arithmetic  8.99 us (2%)
  starting transfers between devices  8.7 us (2%)
  local copies, waits for them, and re-layouts  8.18 us (2%)
    all_gather x1, waiting for transfers between devices, shards(): lax.all_gather(up_weight, 'sp', axis=0, tiled=True)  92.5 us
    all_gather x1, waiting for transfers between devices, shards(): lax.all_gather(down_weight, 'sp', axis=1, tiled=True)  85.1 us
    all_gather x1, waiting for transfers between devices, shards(): lax.all_gather(gate_weight, 'sp', axis=0, tiled=True)  51.4 us
    reduce_scatter x1, waiting for transfers between devices, shards(): lax.psum_scatter(jnp.dot(attention, mine, preferred_element_type=jnp.floa...  37.7 us
    reduce_scatter x1, waiting for transfers between devices, shards(): lax.psum_scatter(terms.astype(jnp.bfloat16), 'tp', scatter_dimension=0, t...  36.2 us
    all_gather x1, waiting for transfers between devices, shards(): normed_all = lax.all_gather(normed, 'tp', axis=0, tiled=True)  28 us
    dot_general x1, matrix products, shards(): jnp.dot(hidden, lax.all_gather(down_weight, 'sp', axis=1, tiled=True), pr...  16.8 us
    dot_general x1, matrix products, shards(): jnp.dot(normed_all, lax.all_gather(gate_weight, 'sp', axis=0, tiled=True)...  9.69 us
  transfers between devices with their start and end apart: 8, of which 6 were waited for; matrix products, arithmetic and copies ran while one was open for 6% of the time, Pallas kernels for 0%

commit v1 on v0

--- a/solution.py
+++ b/solution.py
@@ -1,6 +1,10 @@
+import functools
+
 import jax
 import jax.numpy as jnp
 from jax import lax
+from jax.experimental import pallas as pl
+from jax.experimental.pallas import tpu as pltpu
 from jax.sharding import PartitionSpec as P
 
 HEAD = 64
@@ -100,6 +104,360 @@
     return (mixed.astype(jnp.float32) + ffn).astype(jnp.bfloat16)
 
 
+MESH = pl.DeviceIdType.MESH
+F32 = jnp.float32
+BF16 = jnp.bfloat16
+
+
+def whole_layer(
+    sps, tps, res, q, k, v, sinks, ow, gain, wgu, wd, out,
+    kext, vext, att, abuf, mixed, nbuf, gubuf, dbuf, acc, hid, pbuf, cbuf, sbuf, r1, s1, r2, ssem, rsem,
+):
+    sp, tp = lax.axis_index("sp"), lax.axis_index("tp")
+    g, p = sp // 2, sp % 2
+    x, c = tp // 2, tp % 2
+    groups = sps // 2
+    rows, width = q.shape
+    own, depth = res.shape
+    cut = wd.shape[2]
+    nblk = rows // WINDOW
+    heads = width // HEAD
+    slots = 2 * tps
+    has_l, has_r = g > 0, g < groups - 1
+
+    counter = [0]
+
+    def fresh(n=1):
+        counter[0] += n
+        return counter[0] - n
+
+    def copy(src, dst, ssem_at, rsem_at, to):
+        return pltpu.make_async_remote_copy(
+            src_ref=src, dst_ref=dst, send_sem=ssem.at[ssem_at], recv_sem=rsem.at[rsem_at],
+            device_id=to, device_id_type=MESH,
+        )
+
+    sends = []
+
+    def go(src, dst, rsem_at, to, cond=None):
+        one = copy(src, dst, fresh(), rsem_at, to)
+        sends.append((cond, one))
+        if cond is None:
+            one.start()
+        else:
+            pl.when(cond)(one.start)
+        return one
+
+    left, right = (jnp.maximum(sp - 2, 0), tp), (jnp.minimum(sp + 2, sps - 1), tp)
+    ypeer = (g * 2 + 1 - p, tp)
+    xpeer = (sp, (1 - x) * 2 + c)
+    cpeer = (sp, x * 2 + 1 - c)
+    dpeer = (sp, (1 - x) * 2 + 1 - c)
+    halo_to = (jnp.minimum(sp + 1, sps - 1), tp)
+    halo_from = (jnp.maximum(sp - 1, 0), tp)
+
+    barrier = pltpu.get_barrier_semaphore()
+    for peer in (ypeer, xpeer, cpeer, dpeer):
+        pl.semaphore_signal(barrier, inc=1, device_id=peer, device_id_type=MESH)
+
+    def greet(cond, peer):
+        @pl.when(cond)
+        def _():
+            pl.semaphore_signal(barrier, inc=1, device_id=peer, device_id_type=MESH)
+
+    greet(has_l, left)
+    greet(has_r, right)
+    greet(has_r & (p == 1), halo_to)
+    greet(has_l & (p == 0), halo_from)
+    one = lambda cond: jnp.where(cond, 1, 0)
+    pl.semaphore_wait(
+        barrier, 4 + one(has_l) + one(has_r) + one(has_r & (p == 1)) + one(has_l & (p == 0))
+    )
+
+    R_HK, R_HV, R_YG, R_YD = 0, 1, 2, 3
+    R_GU = 4
+    R_D = R_GU + 2 * groups
+    R_A = R_D + 2 * groups
+    R_N = R_A + 3
+    R_C = R_N + slots
+    R_1 = R_C + 2 * groups
+    R_2 = R_1 + 2 * groups
+
+    first = pl.ds(0, WINDOW)
+    last = pl.ds(rows - WINDOW, WINDOW)
+    halo_k = go(k.at[last], kext.at[first], R_HK, halo_to, sp < sps - 1)
+    halo_v = go(v.at[last], vext.at[first], R_HV, halo_to, sp < sps - 1)
+    go(wgu.at[1 - p], gubuf.at[g, p], R_YG, ypeer)
+    go(wgu.at[p], gubuf.at[g, p], R_GU + 2 * g + p, right, has_r)
+    go(wgu.at[p], gubuf.at[g, p], R_GU + 2 * g + p, left, has_l)
+    go(wd.at[1 - p], dbuf.at[g, p], R_YD, ypeer)
+    gubuf[g, p] = wgu[p]
+    dbuf[g, p] = wd[p]
+
+    def landed(buf, rsem_at):
+        copy(buf, buf, 0, rsem_at, ypeer).wait_recv()
+
+    kext[pl.ds(WINDOW, rows)] = k[...]
+    vext[pl.ds(WINDOW, rows)] = v[...]
+
+    @pl.when(sp == 0)
+    def _():
+        kext[first] = jnp.zeros((WINDOW, HEAD), BF16)
+        vext[first] = jnp.zeros((WINDOW, HEAD), BF16)
+
+    def attend_block(n):
+        at = pl.multiple_of(n * WINDOW, WINDOW)
+        qb = q[pl.ds(at, WINDOW), :]
+        qs = jnp.concatenate([qb[:, h * HEAD : (h + 1) * HEAD] for h in range(heads)], axis=0)
+        kb = kext[pl.ds(at, 2 * WINDOW), :]
+        vb = vext[pl.ds(at, 2 * WINDOW), :]
+        score = lax.dot_general(
+            qs, kb, (((1,), (1,)), ((), ())), preferred_element_type=F32
+        ) * HEAD ** (-0.5)
+        rel = (
+            lax.broadcasted_iota(jnp.int32, score.shape, 0) % WINDOW
+            + WINDOW
+            - lax.broadcasted_iota(jnp.int32, score.shape, 1)
+        )
+        col = lax.broadcasted_iota(jnp.int32, score.shape, 1)
+        start = jnp.where(sp * nblk + n > 0, 0, WINDOW)
+        score = jnp.where((rel >= 0) & (rel < WINDOW) & (col >= start), score, -jnp.inf)
+        sink = jnp.concatenate(
+            [jnp.full((WINDOW, 1), sinks[h], F32) for h in range(heads)], axis=0
+        )
+        top = jnp.maximum(jnp.max(score, axis=-1, keepdims=True), sink)
+        expd = jnp.exp(score - top)
+        denom = jnp.sum(expd, axis=-1, keepdims=True) + jnp.exp(sink - top)
+        weights = (expd / denom).astype(BF16)
+        res_ = jnp.dot(weights, vb, preferred_element_type=F32).astype(BF16)
+        att[pl.ds(at, WINDOW), :] = jnp.concatenate(
+            [res_[h * WINDOW : (h + 1) * WINDOW] for h in range(heads)], axis=1
+        )
+
+    pl.loop(1, nblk)(attend_block)
+    pl.when(sp > 0)(halo_k.wait_recv)
+    pl.when(sp > 0)(halo_v.wait_recv)
+    attend_block(0)
+
+    for i, (peer, who) in enumerate(((xpeer, xpeer[1]), (dpeer, dpeer[1]), (cpeer, cpeer[1]))):
+        go(att.at[pl.ds(pl.multiple_of(who * own, own), own)], abuf.at[i], R_A + i, peer)
+
+    landed(gubuf.at[g, 1 - p], R_YG)
+    go(gubuf.at[g, 1 - p], gubuf.at[g, 1 - p], R_GU + 2 * g + 1 - p, right, has_r)
+    go(gubuf.at[g, 1 - p], gubuf.at[g, 1 - p], R_GU + 2 * g + 1 - p, left, has_l)
+
+    def ow_rows(who):
+        return ow[pl.ds(pl.multiple_of(who * width, width), width), :]
+
+    proj = jnp.dot(
+        att[pl.ds(pl.multiple_of(tp * own, own), own), :], ow_rows(tp), preferred_element_type=F32
+    )
+    acc_p = acc.at[pl.ds(0, own)]
+    for i, who in enumerate((xpeer[1], dpeer[1], cpeer[1])):
+        landed(abuf.at[i], R_A + i)
+        proj += jnp.dot(abuf[i], ow_rows(who), preferred_element_type=F32)
+    mixed[...] = (res[...].astype(F32) + proj).astype(BF16)
+    mixf = mixed[...].astype(F32)
+    normed = (
+        mixf * lax.rsqrt(jnp.mean(mixf * mixf, axis=-1, keepdims=True) + 1e-06) * gain[...]
+    ).astype(BF16)
+
+    def slot(pp, xx, cc):
+        return (pp * 2 + xx) * 2 + cc
+
+    def block(s, lo=0, n=None):
+        return nbuf.at[pl.ds(pl.multiple_of(s * own, own), own), pl.ds(lo, n or depth)]
+
+    mine = slot(p, x, c)
+    nbuf[pl.ds(pl.multiple_of(mine * own, own), own), :] = normed
+    half = depth // 2
+    N_X, N_Y, N_DA, N_DB, N_C = R_N, R_N + 1, R_N + 2, R_N + 3, R_N + 4
+    go(block(mine), block(mine), N_X, xpeer)
+    go(block(mine), block(mine), N_Y, ypeer)
+    go(block(mine), block(mine), N_C, cpeer)
+
+    def order(n):
+        near = jnp.minimum(g, groups - 1 - g)
+        swing = g + (n // 2 if n % 2 == 0 else -((n + 1) // 2))
+        far = jnp.where(g < groups - 1 - g, g + (n - near), g - (n - near))
+        return jnp.where(n <= 2 * near, swing, far)
+
+    def take(buf, base, n, jj):
+        src = order(n)
+        src = jnp.clip(src, 0, groups - 1)
+        landed(buf.at[src, jj], base + 2 * src + jj)
+        onward = ((src < g) & has_r) | ((src > g) & has_l)
+        to = (jnp.where(src < g, right[0], left[0]), tp)
+        go(buf.at[src, jj], buf.at[src, jj], base + 2 * src + jj, to, onward)
+
+    take(gubuf, R_GU, 1, p)
+
+    sx, sy, sd = slot(p, 1 - x, c), slot(1 - p, x, c), slot(1 - p, 1 - x, c)
+    landed(block(sx), N_X)
+    go(block(sx, 0, half), block(sx, 0, half), N_DA, ypeer)
+    go(block(sx), block(sx), N_C + 1, cpeer)
+    landed(block(sy), N_Y)
+    go(block(sy, half, half), block(sy, half, half), N_DB, xpeer)
+    go(block(sy), block(sy), N_C + 2, cpeer)
+    take(gubuf, R_GU, 1, 1 - p)
+    landed(block(sd, 0, half), N_DA)
+    landed(block(sd, half, half), N_DB)
+    go(block(sd), block(sd), N_C + 3, cpeer)
+    landed(block(slot(p, x, 1 - c)), N_C)
+    landed(block(slot(p, 1 - x, 1 - c)), N_C + 1)
+    landed(block(slot(1 - p, x, 1 - c)), N_C + 2)
+    landed(block(slot(1 - p, 1 - x, 1 - c)), N_C + 3)
+
+    def add_block(src, jj, fresh_acc):
+        at = pl.multiple_of((2 * src + jj) * cut, cut)
+
+        @pl.loop(0, slots)
+        def _(i):
+            rs = pl.ds(pl.multiple_of(i * own, own), own)
+            part = lax.dot_general(
+                nbuf[rs, pl.ds(at, cut)], gubuf[src, jj],
+                (((1,), (1,)), ((), ())), preferred_element_type=F32,
+            )
+            if fresh_acc:
+                acc[rs, :] = part
+            else:
+                acc[rs, :] += part
+
+    add_block(g, p, True)
+    add_block(g, 1 - p, False)
+    for n in range(1, groups):
+        src = order(n)
+        for i, jj in enumerate((p, 1 - p)):
+            if n > 1:
+                take(gubuf, R_GU, n, jj)
+            add_block(src, jj, False)
+
+    landed(dbuf.at[g, 1 - p], R_YD)
+    for jj in (0, 1):
+        go(dbuf.at[g, jj], dbuf.at[g, jj], R_D + 2 * g + jj, right, has_r)
+        go(dbuf.at[g, jj], dbuf.at[g, jj], R_D + 2 * g + jj, left, has_l)
+
+    ff = hid.shape[1]
+
+    @pl.loop(0, slots)
+    def _(i):
+        rs = pl.ds(pl.multiple_of(i * own, own), own)
+        both = acc[rs, :]
+        gate, upper = both[:, :ff], both[:, ff:]
+        hid[rs, :] = (jax.nn.silu(gate) * upper).astype(BF16)
+
+    where = []
+
+    def stage0(b):
+        n, jj = b // 2, b % 2
+        src = g if n == 0 else order(n)
+        where.append(2 * src + jj)
+        if n:
+            take(dbuf, R_D, n, jj)
+
+        @pl.loop(0, slots)
+        def _(i):
+            rs = pl.ds(pl.multiple_of(i * own, own), own)
+            part = jnp.dot(hid[rs, :], dbuf[src, jj], preferred_element_type=F32)
+            pbuf[b, i % 2, i // tps, (i // 2) % 2] = part.astype(BF16)
+
+        go(pbuf.at[b, 1 - c], cbuf.at[b], R_C + b, cpeer)
+
+    def stage1(b):
+        landed(cbuf.at[b], R_C + b)
+        sbuf[b] = (pbuf[b, c].astype(F32) + cbuf[b].astype(F32)).astype(BF16)
+        if b % 2 == 0:
+            go(sbuf.at[b, :, 1 - x], r1.at[b], R_1 + b, xpeer)
+        else:
+            go(sbuf.at[b, 1 - p], r1.at[b], R_1 + b, ypeer)
+
+    def stage2(b):
+        landed(r1.at[b], R_1 + b)
+        kept = sbuf[b, :, x] if b % 2 == 0 else sbuf[b, p]
+        s1[b] = (kept.astype(F32) + r1[b].astype(F32)).astype(BF16)
+        if b % 2 == 0:
+            go(s1.at[b, 1 - p], r2.at[b], R_2 + b, ypeer)
+        else:
+            go(s1.at[b, 1 - x], r2.at[b], R_2 + b, xpeer)
+
+    def stage3(b):
+        landed(r2.at[b], R_2 + b)
+        kept = s1[b, p] if b % 2 == 0 else s1[b, x]
+        cols = pl.ds(pl.multiple_of(where[b] * cut, cut), cut)
+        out[:, cols] = (
+            mixed[:, cols].astype(F32) + (kept.astype(F32) + r2[b].astype(F32))
+        ).astype(BF16)
+
+    stages = (stage0, stage1, stage2, stage3)
+    total = 2 * groups
+    for step in range(total + 3):
+        for i, stage in enumerate(stages):
+            if 0 <= step - i < total:
+                stage(step - i)
+
+    for cond, one_copy in sends:
+        if cond is None:
+            one_copy.wait_send()
+        else:
+            pl.when(cond)(one_copy.wait_send)
+
+
+def layer(
+    sps, tps, residual, queries, keys, values, sinks, out_weight, norm_gain,
+    gate_weight, up_weight, down_weight,
+):
+    rows, width = queries.shape
+    own, depth = residual.shape
+    blk, ff = gate_weight.shape
+    fits = (
+        sps % 2 == 0 and 4 <= sps <= 8 and tps == 4 and keys.shape[1] == HEAD
+        and blk % 128 == 0 and ff % 32 == 0 and own % 16 == 0
+    )
+    if not fits:
+        return shards(
+            residual, queries, keys, values, sinks, out_weight, norm_gain,
+            gate_weight, up_weight, down_weight,
+        )
+    groups, ffh, slots = sps // 2, ff // 2, 2 * tps
+    wgu = jnp.concatenate(
+        [gate_weight.T.reshape(2, ffh, blk), up_weight.T.reshape(2, ffh, blk)], axis=1
+    )
+    wd = down_weight.reshape(2, ffh, blk)
+    vm = pl.BlockSpec(memory_space=pltpu.VMEM)
+    sm = pl.BlockSpec(memory_space=pltpu.SMEM)
+    nb = 2 * groups
+    return pl.pallas_call(
+        functools.partial(whole_layer, sps, tps),
+        out_shape=jax.ShapeDtypeStruct((own, depth), BF16),
+        in_specs=[vm] * 4 + [sm] + [vm] * 4,
+        out_specs=vm,
+        scratch_shapes=[
+            pltpu.VMEM((rows + WINDOW, HEAD), BF16),
+            pltpu.VMEM((rows + WINDOW, HEAD), BF16),
+            pltpu.VMEM((rows, width), BF16),
+            pltpu.VMEM((3, own, width), BF16),
+            pltpu.VMEM((own, depth), BF16),
+            pltpu.VMEM((slots * own, depth), BF16),
+            pltpu.VMEM((groups, 2, 2 * ffh, blk), BF16),
+            pltpu.VMEM((groups, 2, ffh, blk), BF16),
+            pltpu.VMEM((slots * own, 2 * ffh), F32),
+            pltpu.VMEM((slots * own, ffh), BF16),
+            pltpu.VMEM((nb, 2, 2, 2, own, blk), BF16),
+            pltpu.VMEM((nb, 2, 2, own, blk), BF16),
+            pltpu.VMEM((nb, 2, 2, own, blk), BF16),
+            pltpu.VMEM((nb, 2, own, blk), BF16),
+            pltpu.VMEM((nb, 2, own, blk), BF16),
+            pltpu.VMEM((nb, own, blk), BF16),
+            pltpu.SemaphoreType.DMA((24 * groups + 48,)),
+            pltpu.SemaphoreType.DMA((24 * groups + 48,)),
+        ],
+        compiler_params=pltpu.CompilerParams(
+            collective_id=0, has_side_effects=True, vmem_limit_bytes=66000000
+        ),
+        name="whole_layer",
+    )(residual, queries, keys, values, sinks, out_weight, norm_gain.reshape(1, depth), wgu, wd)
+
+
 def solution(mesh):
     placed = (
         P(("sp", "tp"), None),
@@ -114,5 +472,5 @@
         P("tp", "sp"),
     )
     return jax.shard_map(
-        shards, mesh=mesh, in_specs=placed, out_specs=P(("sp", "tp"), None), check_vma=False
-    )
+        functools.partial(layer, mesh.shape["sp"], mesh.shape["tp"]), mesh=mesh, in_specs=placed, out_specs=P(("sp", "tp"), None), check_vma=False
+    )

time: 409 us -> 221 us (0.54)
  waiting for transfers between devices: 333 us -> 0 us
  Pallas kernels: 0 us -> 213 us
  matrix products: 34.1 us -> 0 us
  between operations: 15.2 us -> 0.02 us
  starting transfers between devices: 8.7 us -> 0 us
  other arithmetic: 8.99 us -> 1.22 us
    all_gather x4 -> x0, waiting for transfers between devices: 257 us -> none  [the longest x1 92.5 us: shards(): lax.all_gather(up_weight, 'sp', axis=0, tiled=True)]
    pallas_call x0 -> x1, Pallas kernels: none -> 213 us  [layer(): pl.pallas_call(functools.partial(whole_layer, sps, tps), out_shape=jax.Sh...]
    reduce_scatter x2 -> x0, waiting for transfers between devices: 73.8 us -> none  [the longest x1 37.7 us: shards(): lax.psum_scatter(jnp.dot(attention, mine, preferred_element_type=jnp.floa...]
    dot_general x5 -> x0, matrix products: 34.1 us -> none  [the longest x1 16.8 us: shards(): jnp.dot(hidden, lax.all_gather(down_weight, 'sp', axis=1, tiled=True), pr...]
    ppermute x2 -> x0, starting transfers between devices: 8.3 us -> none  [passed_along(): return lax.ppermute(block, axis, route)]
    convert_element_type x2 -> x0, other arithmetic: 4.71 us -> none  [the longest x1 2.4 us: shards(): return (mixed.astype(jnp.float32) + ffn).astype(jnp.bfloat16)]
  transfers between devices with their start and end apart: 8 -> 0, of which waited for: 6 -> 0; matrix products, arithmetic and copies ran while one was open for 6% -> 0% of each run, Pallas kernels for 0% -> 0%
where the time goes in v1:
time: 221 us
  Pallas kernels  213 us (96%)
  local copies, waits for them, and re-layouts  6.52 us (3%)
    pallas_call x1, Pallas kernels, layer(): pl.pallas_call(functools.partial(whole_layer, sps, tps), out_shape=jax.Sh...  213 us

profile of v1, /device:TPU:0, one launch (start us, length us, event | category | flops | bytes accessed | tf_op | source)
XLA Modules:
  0.0 220.5 jit_solution(7362616138144494229)
XLA Ops:
  0.0 0.0 copy-start
  0.0 0.0 copy-start.1
  0.0 1.4 copy.11
  1.4 1.4 copy.12
  2.8 1.2 pad_maximum_fusion.wgu
  4.0 0.0 copy-done
  4.0 0.8 copy.13.k
  4.8 0.0 copy-done.1
  4.8 0.8 copy.14.v
  5.7 212.8 %whole_layer.1 = bf16[192,2048]{1,0:T(8,128)(2,1)} custom-call(bf16[192,2048]{1,0:T(8,128)(2,1)} %res.1, bf16[768,256]{1,0:T(8,128)(2,1)} %q.1, bf16[768,64]{1,0:T(8,128)(2,1)} %copy.13.k, bf16[768,64]{1,0:T(8,128)(2,1)} %copy.14.v, f32[4]{0:T(128)} %sinks.1, bf16[1024,2048]{1,0:T(8,128)(2,1)} %ow.1, f32[1,2048]{1,0:T(1,128)} %bitcast.11, ...), custom_call_target="tpu_custom_call" | custom-call | tf_op jit(solution)/shard_map/whole_layer/pallas_call | solution.py:429
  218.4 2.1 copy.16
Async XLA Ops:
  0.0 4.0 %copy-start = (bf16[768,64]{0,1:T(8,128)(2,1)S(1)}, bf16[768,64]{0,1:T(8,128)(2,1)}, u32[]{:S(2)}) copy-start(bf16[768,64]{0,1:T(8,128)(2,1)} %param.12) | copy-start | bytes 294916
  0.0 4.8 %copy-start.1 = (bf16[768,64]{0,1:T(8,128)(2,1)S(1)}, bf16[768,64]{0,1:T(8,128)(2,1)}, u32[]{:S(2)}) copy-start(bf16[768,64]{0,1:T(8,128)(2,1)} %param.13) | copy-start | bytes 294916

commit v2 on v1

--- a/solution.py
+++ b/solution.py
@@ -191,6 +191,8 @@
     go(wgu.at[p], gubuf.at[g, p], R_GU + 2 * g + p, right, has_r)
     go(wgu.at[p], gubuf.at[g, p], R_GU + 2 * g + p, left, has_l)
     go(wd.at[1 - p], dbuf.at[g, p], R_YD, ypeer)
+    for side, cond in ((right, has_r), (left, has_l)):
+        go(wd.at[p], dbuf.at[g, p], R_D + 2 * g + p, side, cond)
     gubuf[g, p] = wgu[p]
     dbuf[g, p] = wd[p]
 
@@ -234,7 +236,12 @@
             [res_[h * WINDOW : (h + 1) * WINDOW] for h in range(heads)], axis=1
         )
 
-    pl.loop(1, nblk)(attend_block)
+    pl.loop(1, nblk // 2)(attend_block)
+
+    landed(gubuf.at[g, 1 - p], R_YG)
+    for side, cond in ((right, has_r), (left, has_l)):
+        go(gubuf.at[g, 1 - p], gubuf.at[g, 1 - p], R_GU + 2 * g + 1 - p, side, cond)
+    pl.loop(nblk // 2, nblk)(attend_block)
     pl.when(sp > 0)(halo_k.wait_recv)
     pl.when(sp > 0)(halo_v.wait_recv)
     attend_block(0)
@@ -242,9 +249,9 @@
     for i, (peer, who) in enumerate(((xpeer, xpeer[1]), (dpeer, dpeer[1]), (cpeer, cpeer[1]))):
         go(att.at[pl.ds(pl.multiple_of(who * own, own), own)], abuf.at[i], R_A + i, peer)
 
-    landed(gubuf.at[g, 1 - p], R_YG)
-    go(gubuf.at[g, 1 - p], gubuf.at[g, 1 - p], R_GU + 2 * g + 1 - p, right, has_r)
-    go(gubuf.at[g, 1 - p], gubuf.at[g, 1 - p], R_GU + 2 * g + 1 - p, left, has_l)
+    landed(dbuf.at[g, 1 - p], R_YD)
+    for side, cond in ((right, has_r), (left, has_l)):
+        go(dbuf.at[g, 1 - p], dbuf.at[g, 1 - p], R_D + 2 * g + 1 - p, side, cond)
 
     def ow_rows(who):
         return ow[pl.ds(pl.multiple_of(who * width, width), width), :]
@@ -282,24 +289,51 @@
         far = jnp.where(g < groups - 1 - g, g + (n - near), g - (n - near))
         return jnp.where(n <= 2 * near, swing, far)
 
-    def take(buf, base, n, jj):
-        src = order(n)
-        src = jnp.clip(src, 0, groups - 1)
-        landed(buf.at[src, jj], base + 2 * src + jj)
-        onward = ((src < g) & has_r) | ((src > g) & has_l)
-        to = (jnp.where(src < g, right[0], left[0]), tp)
-        go(buf.at[src, jj], buf.at[src, jj], base + 2 * src + jj, to, onward)
-
-    take(gubuf, R_GU, 1, p)
+    other = 1 - p
+    arrivals = {}
+    for base, buf in ((R_GU, gubuf), (R_D, dbuf)):
+        for n in range(1, groups):
+            src = jnp.clip(order(n), 0, groups - 1)
+            onward = ((src < g) & has_r) | ((src > g) & has_l)
+            to = (jnp.where(src < g, right[0], left[0]), tp)
+            for jj in (p, other):
+                ref, at = buf.at[src, jj], base + 2 * src + jj
+                hop = copy(ref, ref, fresh(), at, to)
+                sends.append((onward, hop))
+                arrivals[base, n, jj is p] = (onward, copy(ref, ref, 0, at, ypeer), hop)
+
+    def take(base, n, jj, cond=None):
+        onward, arrived, hop = arrivals[base, n, jj is p]
+        if cond is None:
+            arrived.wait_recv()
+            pl.when(onward)(hop.start)
+        else:
+            pl.when(cond)(arrived.wait_recv)
+            pl.when(cond & onward)(hop.start)
+
+    near = jnp.minimum(g, groups - 1 - g)
+    early = groups - 2
+
+    def take_early(base, jj):
+        take(base, 1, jj)
+        for n in range(2, early + 1):
+            take(base, n, jj, n <= 2 * near)
+
+    def take_late(base, n, jj):
+        if n > early:
+            take(base, n, jj)
+        elif n > 1:
+            take(base, n, jj, n > 2 * near)
 
     sx, sy, sd = slot(p, 1 - x, c), slot(1 - p, x, c), slot(1 - p, 1 - x, c)
+    take_early(R_GU, p)
     landed(block(sx), N_X)
     go(block(sx, 0, half), block(sx, 0, half), N_DA, ypeer)
     go(block(sx), block(sx), N_C + 1, cpeer)
     landed(block(sy), N_Y)
     go(block(sy, half, half), block(sy, half, half), N_DB, xpeer)
     go(block(sy), block(sy), N_C + 2, cpeer)
-    take(gubuf, R_GU, 1, 1 - p)
+    take_early(R_GU, other)
     landed(block(sd, 0, half), N_DA)
     landed(block(sd, half, half), N_DB)
     go(block(sd), block(sd), N_C + 3, cpeer)
@@ -327,15 +361,12 @@
     add_block(g, 1 - p, False)
     for n in range(1, groups):
         src = order(n)
-        for i, jj in enumerate((p, 1 - p)):
-            if n > 1:
-                take(gubuf, R_GU, n, jj)
+        for jj in (p, other):
+            take_late(R_GU, n, jj)
+            if n == groups - 1 and jj is other:
+                for dj in (p, other):
+                    take_early(R_D, dj)
             add_block(src, jj, False)
-
-    landed(dbuf.at[g, 1 - p], R_YD)
-    for jj in (0, 1):
-        go(dbuf.at[g, jj], dbuf.at[g, jj], R_D + 2 * g + jj, right, has_r)
-        go(dbuf.at[g, jj], dbuf.at[g, jj], R_D + 2 * g + jj, left, has_l)
 
     ff = hid.shape[1]
 
@@ -352,8 +383,9 @@
         n, jj = b // 2, b % 2
         src = g if n == 0 else order(n)
         where.append(2 * src + jj)
-        if n:
-            take(dbuf, R_D, n, jj)
+        if n > 1 and jj == 0:
+            for dj in (p, other):
+                take_late(R_D, n, dj)
 
         @pl.loop(0, slots)
         def _(i):

time: 221 us -> 185 us (0.84)
  Pallas kernels: 213 us -> 177 us
    pallas_call x1, Pallas kernels: 213 us -> 177 us  [layer(): pl.pallas_call(functools.partial(whole_layer, sps, tps), out_shape=jax.Sh...]
where the time goes in v2:
time: 185 us
  Pallas kernels  177 us (96%)
  local copies, waits for them, and re-layouts  6.52 us (4%)
    pallas_call x1, Pallas kernels, layer(): pl.pallas_call(functools.partial(whole_layer, sps, tps), out_shape=jax.Sh...  177 us
    unnamed x7, local copies, waits for them, and re-layouts  3.72 us

profile of v2, /device:TPU:0, one launch (start us, length us, event | category | flops | bytes accessed | tf_op | source)
XLA Modules:
  0.0 184.8 jit_solution(8909313818847335172)
XLA Ops:
  0.0 0.0 copy-start
  0.0 0.0 copy-start.1
  0.0 1.4 copy.11
  1.4 1.4 copy.12
  2.8 1.2 pad_maximum_fusion.wgu
  4.0 0.0 copy-done
  4.0 0.8 copy.13.k
  4.8 0.0 copy-done.1
  4.8 0.8 copy.14.v
  5.7 177.0 %whole_layer.1 = bf16[192,2048]{1,0:T(8,128)(2,1)} custom-call(bf16[192,2048]{1,0:T(8,128)(2,1)} %res.1, bf16[768,256]{1,0:T(8,128)(2,1)} %q.1, bf16[768,64]{1,0:T(8,128)(2,1)} %copy.13.k, bf16[768,64]{1,0:T(8,128)(2,1)} %copy.14.v, f32[4]{0:T(128)} %sinks.1, bf16[1024,2048]{1,0:T(8,128)(2,1)} %ow.1, f32[1,2048]{1,0:T(1,128)} %bitcast.11, ...), custom_call_target="tpu_custom_call" | custom-call | tf_op jit(solution)/shard_map/whole_layer/pallas_call | solution.py:461
  182.7 2.1 %copy.16 = bf16[192,2048]{1,0:T(8,128)(2,1)} copy(bf16[192,2048]{1,0:T(8,128)(2,1)} %whole_layer.1) | data formatting | bytes 1572864
Async XLA Ops:
  0.0 4.0 %copy-start = (bf16[768,64]{0,1:T(8,128)(2,1)S(1)}, bf16[768,64]{0,1:T(8,128)(2,1)}, u32[]{:S(2)}) copy-start(bf16[768,64]{0,1:T(8,128)(2,1)} %param.12) | copy-start | bytes 294916
  0.0 4.8 %copy-start.1 = (bf16[768,64]{0,1:T(8,128)(2,1)S(1)}, bf16[768,64]{0,1:T(8,128)(2,1)}, u32[]{:S(2)}) copy-start(bf16[768,64]{0,1:T(8,128)(2,1)} %param.13) | copy-start | bytes 294916

commit v3 on v2

--- a/solution.py
+++ b/solution.py
@@ -110,8 +110,8 @@
 
 
 def whole_layer(
-    sps, tps, res, q, k, v, sinks, ow, gain, wgu, wd, out,
-    kext, vext, att, abuf, mixed, nbuf, gubuf, dbuf, acc, hid, pbuf, cbuf, sbuf, r1, s1, r2, ssem, rsem,
+    sps, tps, res, q, k, v, sinks, ow_hbm, gain, wgu, wd, out,
+    kext, vext, att, abuf, mixed, nbuf, gubuf, dbuf, acc, hid, pbuf, cbuf, sbuf, r1, s1, r2, ow, osem, ssem, rsem,
 ):
     sp, tp = lax.axis_index("sp"), lax.axis_index("tp")
     g, p = sp // 2, sp % 2
@@ -193,6 +193,8 @@
     go(wd.at[1 - p], dbuf.at[g, p], R_YD, ypeer)
     for side, cond in ((right, has_r), (left, has_l)):
         go(wd.at[p], dbuf.at[g, p], R_D + 2 * g + p, side, cond)
+    fetch = pltpu.make_async_copy(ow_hbm, ow, osem)
+    fetch.start()
     gubuf[g, p] = wgu[p]
     dbuf[g, p] = wd[p]
 
@@ -256,6 +258,7 @@
     def ow_rows(who):
         return ow[pl.ds(pl.multiple_of(who * width, width), width), :]
 
+    fetch.wait()
     proj = jnp.dot(
         att[pl.ds(pl.multiple_of(tp * own, own), own), :], ow_rows(tp), preferred_element_type=F32
     )
@@ -291,19 +294,20 @@
 
     other = 1 - p
     arrivals = {}
+    key = lambda jj: jj if isinstance(jj, int) else jj is p
     for base, buf in ((R_GU, gubuf), (R_D, dbuf)):
         for n in range(1, groups):
             src = jnp.clip(order(n), 0, groups - 1)
             onward = ((src < g) & has_r) | ((src > g) & has_l)
             to = (jnp.where(src < g, right[0], left[0]), tp)
-            for jj in (p, other):
+            for jj in (p, other) if base == R_GU else (0, 1):
                 ref, at = buf.at[src, jj], base + 2 * src + jj
                 hop = copy(ref, ref, fresh(), at, to)
                 sends.append((onward, hop))
-                arrivals[base, n, jj is p] = (onward, copy(ref, ref, 0, at, ypeer), hop)
+                arrivals[base, n, key(jj)] = (onward, copy(ref, ref, 0, at, ypeer), hop)
 
     def take(base, n, jj, cond=None):
-        onward, arrived, hop = arrivals[base, n, jj is p]
+        onward, arrived, hop = arrivals[base, n, key(jj)]
         if cond is None:
             arrived.wait_recv()
             pl.when(onward)(hop.start)
@@ -364,7 +368,7 @@
         for jj in (p, other):
             take_late(R_GU, n, jj)
             if n == groups - 1 and jj is other:
-                for dj in (p, other):
+                for dj in (0, 1):
                     take_early(R_D, dj)
             add_block(src, jj, False)
 
@@ -383,9 +387,8 @@
         n, jj = b // 2, b % 2
         src = g if n == 0 else order(n)
         where.append(2 * src + jj)
-        if n > 1 and jj == 0:
-            for dj in (p, other):
-                take_late(R_D, n, dj)
+        if n > 1:
+            take_late(R_D, n, jj)
 
         @pl.loop(0, slots)
         def _(i):
@@ -461,7 +464,7 @@
     return pl.pallas_call(
         functools.partial(whole_layer, sps, tps),
         out_shape=jax.ShapeDtypeStruct((own, depth), BF16),
-        in_specs=[vm] * 4 + [sm] + [vm] * 4,
+        in_specs=[vm] * 4 + [sm, pl.BlockSpec(memory_space=pl.ANY)] + [vm] * 3,
         out_specs=vm,
         scratch_shapes=[
             pltpu.VMEM((rows + WINDOW, HEAD), BF16),
@@ -480,6 +483,8 @@
             pltpu.VMEM((nb, 2, own, blk), BF16),
             pltpu.VMEM((nb, 2, own, blk), BF16),
             pltpu.VMEM((nb, own, blk), BF16),
+            pltpu.VMEM(out_weight.shape, BF16),
+            pltpu.SemaphoreType.DMA,
             pltpu.SemaphoreType.DMA((24 * groups + 48,)),
             pltpu.SemaphoreType.DMA((24 * groups + 48,)),
         ],

time: 185 us -> 182 us (0.984)
  Pallas kernels: 177 us -> 174 us
    pallas_call x1, Pallas kernels: 177 us -> 174 us  [layer(): pl.pallas_call(functools.partial(whole_layer, sps, tps), out_shape=jax.Sh...]
where the time goes in v3:
time: 182 us; the launch traced here: 181 us
  Pallas kernels  174 us (96%)
  local copies, waits for them, and re-layouts  6.52 us (4%)
    pallas_call x1, Pallas kernels, layer(): pl.pallas_call(functools.partial(whole_layer, sps, tps), out_shape=jax.Sh...  174 us
    unnamed x7, local copies, waits for them, and re-layouts  3.72 us

profile of v3, /device:TPU:0, one launch (start us, length us, event | category | flops | bytes accessed | tf_op | source)
XLA Modules:
  0.0 181.5 jit_solution(17949821238790814769)
XLA Ops:
  0.0 0.0 copy-start
  0.0 0.0 copy-start.1
  0.0 1.4 copy.11
  1.4 1.4 copy.12
  2.8 1.2 pad_maximum_fusion.wgu
  4.0 0.0 copy-done
  4.0 0.8 copy.13.k
  4.8 0.0 copy-done.1
  4.8 0.8 copy.14.v
  5.7 173.7 %whole_layer.1 = bf16[192,2048]{1,0:T(8,128)(2,1)} custom-call(bf16[192,2048]{1,0:T(8,128)(2,1)} %res.1, bf16[768,256]{1,0:T(8,128)(2,1)} %q.1, bf16[768,64]{1,0:T(8,128)(2,1)} %copy.13.k, bf16[768,64]{1,0:T(8,128)(2,1)} %copy.14.v, f32[4]{0:T(128)} %sinks.1, bf16[1024,2048]{1,0:T(8,128)(2,1)} %ow_hbm.1, f32[1,2048]{1,0:T(1,128)} %bitcast.11, ...), custom_call_target="tpu_custom_call" | custom-call | tf_op jit(solution)/shard_map/whole_layer/pallas_call | solution.py:464
  179.4 2.1 %copy.16 = bf16[192,2048]{1,0:T(8,128)(2,1)} copy(bf16[192,2048]{1,0:T(8,128)(2,1)} %whole_layer.1) | data formatting | bytes 1572864
Async XLA Ops:
  0.0 4.0 %copy-start = (bf16[768,64]{0,1:T(8,128)(2,1)S(1)}, bf16[768,64]{0,1:T(8,128)(2,1)}, u32[]{:S(2)}) copy-start(bf16[768,64]{0,1:T(8,128)(2,1)} %param.12) | copy-start | bytes 294916
  0.0 4.8 %copy-start.1 = (bf16[768,64]{0,1:T(8,128)(2,1)S(1)}, bf16[768,64]{0,1:T(8,128)(2,1)}, u32[]{:S(2)}) copy-start(bf16[768,64]{0,1:T(8,128)(2,1)} %param.13) | copy-start | bytes 294916
